TPU v7x, 512 devices: a whole 4x8x8 slice. The times are simulated.
512 devices in a mesh: sp: 64 (over z, y), fs: 4 (over x), tp: 2 (over core).
Axes of the slice: x: 4, y: 8, z: 8, core: 2. Of those that a mesh axis runs over, the one named last changes fastest.
Arguments:
- tokens: bfloat16 [32768, 2048], P(('fs', 'sp')), may hold values from -6 to 6
- in_gain: float32 [2048], replicated, may hold values from 0.1 to 1.9
- query_weight: bfloat16 [2048, 512], P(None, ('tp', 'fs')), may hold values from -0.17291713 to 0.17291713
- key_weight: bfloat16 [2048, 512], P(None, ('tp', 'fs')), may hold values from -0.17291713 to 0.17291713
- value_weight: bfloat16 [2048, 512], P(None, ('tp', 'fs')), may hold values from -0.125 to 0.125
- rec_query_weight: bfloat16 [2048, 512], P(None, ('tp', 'fs')), may hold values from -0.125 to 0.125
- rec_forget_weight: bfloat16 [2048, 512], P(None, ('tp', 'fs')), may hold values from -0.125 to 0.125
- rec_input_weight: bfloat16 [2048, 512], P(None, ('tp', 'fs')), may hold values from -0.125 to 0.125
- mix_lambda: float32 [4], P('tp'), may hold values from 0.3 to 0.8
- lower_bound: float32 [4, 128], P('tp'), may hold values from 0.9 to 0.9999695
- forget_scale: float32 [32768], P(('fs', 'sp')), may hold values from 0.35 to 24576
- att_gain: float32 [128], replicated, may hold values from 0.1 to 1.9
- recurrence_gain: float32 [128], replicated, may hold values from 0.1 to 1.9
- att_out_weight: bfloat16 [512, 2048], P('tp'), may hold values from -0.1875 to 0.1875
- rec_out_weight: bfloat16 [512, 2048], P('tp'), may hold values from -0.1875 to 0.1875
Outputs:
- mixed_out: bfloat16 [32768, 2048], P(('fs', 'sp'))
- log_weight_sum: float32 [4, 32768], P('tp', ('fs', 'sp'))
All inputs are finite; a program needn't handle non-finite values.
Results may differ from a plain program's by a relative error of at most 0.012.
Values may be sent and summed in bfloat16 or wider, within the bound.
No kernel may reach another device: no remote copies, remote signals or barrier semaphores. Data moves between devices by JAX's collectives and lax.ppermute only.
A program may use at most 128 MiB of HBM per device.

v0:
```python
import jax
import jax.numpy as jnp
from jax import lax
from jax.sharding import Mesh
from jax.sharding import PartitionSpec as P

DK = 64
DV = 128
BLK = 64
SP = ("sp_0", "sp_1")
FS_SP = ("fs", "sp_0", "sp_1")


EPS = 1e-06
NEG = -1e30


def in_one_piece(arrays, axis, dim, along):
    widths = [a.shape[along] for a in arrays]
    both = jnp.concatenate(arrays, axis=along)
    filled = lax.all_gather(both, axis, axis=dim, tiled=True)
    return tuple(jnp.split(filled, [sum(widths[:k]) for k in range(1, len(widths))], axis=along))


def nothing_yet(x, identity):
    return jax.tree.map(
        lambda part, zero: jnp.zeros_like(part) + jnp.asarray(zero, part.dtype), x, identity
    )


def entering(x, axes, combine, identity):
    before = start = nothing_yet(x, identity)
    running = x
    for axis in reversed(axes):
        peers, here = (lax.axis_size(axis), lax.axis_index(axis))
        pieces = jax.tree.map(lambda part: lax.all_gather(part, axis), running)
        inside, running = (start, start)
        for k in range(peers):
            passed = k < here
            running = combine(running, jax.tree.map(lambda part: part[k], pieces))
            inside = jax.tree.map(lambda new, old: jnp.where(passed, new, old), running, inside)
        before = combine(inside, before)
    return before


def copy_for_each(x, axis):
    peers = lax.axis_size(axis)
    return lax.all_to_all(jnp.broadcast_to(x[None], (peers, *x.shape)), axis, 0, 0, tiled=True)


def taken_together(x, axis):
    return copy_for_each(x, axis).astype(jnp.float32).sum(axis=0)


def norm_rows(values, gain):
    return values * lax.rsqrt(jnp.mean(values * values, axis=-1, keepdims=True) + EPS) * gain


def block_recurrence(queries, key_in, value_in, log_forget):
    head_count, row_count, key_width = queries.shape
    block_count = row_count // BLK

    def to_blocks(array_in):
        return array_in.reshape(head_count, block_count, BLK, array_in.shape[-1]).transpose(
            1, 0, 2, 3
        )

    causal = jnp.tril(jnp.ones((BLK, BLK), bool))

    def advance(passed_state, inputs):
        query_block, key_block, value_block, l_blk = inputs
        accumulator_sum = jnp.cumsum(l_blk, axis=1)
        cross_block_output = jnp.einsum(
            "sre,sei->sri",
            query_block * jnp.exp(accumulator_sum),
            passed_state,
            precision=lax.Precision.HIGHEST,
        )
        spread = accumulator_sum[:, :, None, :] - accumulator_sum[:, None, :, :]
        decay = jnp.exp(jnp.where(causal[None, :, :, None], spread, -jnp.inf))
        scores = jnp.einsum(
            "htk,htsk,hsk->hts", query_block, decay, key_block, precision=lax.Precision.HIGHEST
        )
        result = cross_block_output + jnp.einsum(
            "hts,hsv->htv", scores, value_block, precision=lax.Precision.HIGHEST
        )
        final_log_sum = accumulator_sum[:, -1:, :]
        updated_state = jnp.exp(final_log_sum[:, 0, :])[:, :, None] * passed_state + jnp.einsum(
            "plf,plt->pft",
            key_block * jnp.exp(final_log_sum - accumulator_sum),
            value_block,
            precision=lax.Precision.HIGHEST,
        )
        return (updated_state, result)

    begin_state = jnp.zeros((head_count, key_width, value_in.shape[-1]), jnp.float32)
    end_state, results = lax.scan(
        advance,
        begin_state,
        (to_blocks(queries), to_blocks(key_in), to_blocks(value_in), to_blocks(log_forget)),
    )
    return (
        end_state,
        results.transpose(1, 0, 2, 3).reshape(head_count, row_count, value_in.shape[-1]),
    )


def attend(online, queries, pair_keys, pair_values, allowed):
    running_max, weight_sum, numer_sum = online
    local_heads = numer_sum.shape[0]
    key_rows = pair_keys.shape[0]
    key_heads = pair_keys.reshape(key_rows, local_heads, 2, DK).transpose(1, 2, 0, 3)
    head_values = pair_values.reshape(key_rows, local_heads, DV).transpose(1, 0, 2)
    scores = jnp.einsum(
        "hmqd,hmkd->hmqk", queries, key_heads, preferred_element_type=jnp.float32
    ) * DK ** (-0.5)
    scores = jnp.where(allowed, scores, NEG)
    highest = jnp.maximum(running_max, jnp.max(scores, axis=-1))
    weights = jnp.exp(scores - highest[..., None])
    weight_sum = jnp.sum(weights, axis=-1)
    numer_sum = jnp.einsum(
        "itap,ipn->itan",
        weights.astype(jnp.bfloat16),
        head_values,
        preferred_element_type=jnp.float32,
    )
    return (highest, weight_sum, numer_sum)


def on_device(
    tokens,
    in_gain,
    query_weight,
    key_weight,
    value_weight,
    rec_query_weight,
    rec_forget_weight,
    rec_input_weight,
    mix_lambda,
    lower_bound,
    forget_scale,
    att_gain,
    recurrence_gain,
    att_out_weight,
    rec_out_weight,
):
    normed = norm_rows(tokens.astype(jnp.float32), in_gain).astype(jnp.bfloat16)
    row_count = normed.shape[0]
    stacked = jnp.stack(
        [
            query_weight,
            key_weight,
            value_weight,
            rec_query_weight,
            rec_forget_weight,
            rec_input_weight,
        ],
        axis=1,
    )
    projected = jnp.einsum(
        "rd,dnc->rnc",
        normed,
        lax.all_gather(stacked, "fs", axis=2, tiled=True),
        preferred_element_type=jnp.float32,
    ).astype(jnp.bfloat16)
    local_heads = projected.shape[2] // DV
    position = lax.axis_index(SP)
    query_pos = position * row_count + jnp.arange(row_count)
    queries = projected[:, 0].reshape(row_count, local_heads, 2, DK).transpose(1, 2, 0, 3)
    online = (
        jnp.full((local_heads, 2, row_count), NEG, jnp.float32),
        jnp.zeros((local_heads, 2, row_count), jnp.float32),
        jnp.zeros((local_heads, 2, row_count, DV), jnp.float32),
    )
    pair_keys, pair_values = in_one_piece((projected[:, 1], projected[:, 2]), SP, 0, 1)
    key_pos = jnp.arange(pair_keys.shape[0])
    allowed = query_pos[:, None] >= key_pos[None, :]
    online = lax.cond(
        jnp.int32(0) <= query_pos[-1],
        lambda state: attend(state, queries, pair_keys, pair_values, allowed),
        lambda state: state,
        online,
    )
    running_max, weight_sum, numer_sum = online
    mixed_heads = (
        numer_sum[:, 0] / weight_sum[:, 0, :, None]
        - mix_lambda[:, None, None] * numer_sum[:, 1] / weight_sum[:, 1, :, None]
    )
    att_heads = (norm_rows(mixed_heads, att_gain) * 0.8).astype(jnp.bfloat16)
    att_rows = att_heads.transpose(1, 0, 2).reshape(row_count, local_heads * DV)
    log_weight_sum = running_max[:, 0] + jnp.log(weight_sum[:, 0])

    def heads_first(array_in):
        return array_in.reshape(row_count, local_heads, DV).transpose(1, 0, 2).astype(jnp.float32)

    recurrent_queries = heads_first(projected[:, 3])
    lower_edge = lower_bound[:, None, :]
    forget = lower_edge + (1.0 - lower_edge) * jax.nn.sigmoid(heads_first(projected[:, 4]))
    log_forget = forget_scale[None, :, None] * jnp.log(forget)
    key_in = 1.0 - jnp.exp(log_forget)
    end_state, local_result = block_recurrence(
        recurrent_queries, key_in, heads_first(projected[:, 5]), log_forget
    )
    running_state = jnp.cumsum(log_forget, axis=1)
    carry_rate = jnp.exp(running_state[:, -1, :])

    def combine(earlier, later):
        return (later[0] * earlier[0], later[0][..., None] * earlier[1] + later[1])

    identity = (jnp.ones_like(carry_rate), jnp.zeros_like(end_state))
    _, incoming_state = entering((carry_rate, end_state), SP, combine, identity)
    combined = local_result + jnp.einsum(
        "zed,zdp->zep",
        recurrent_queries * jnp.exp(running_state),
        incoming_state,
        precision=lax.Precision.HIGHEST,
    )
    rec_heads = norm_rows(combined, recurrence_gain).astype(jnp.bfloat16)
    rec_rows = rec_heads.transpose(1, 0, 2).reshape(row_count, local_heads * DV)
    partial_value = jnp.dot(att_rows, att_out_weight, preferred_element_type=jnp.float32) + jnp.dot(
        rec_rows, rec_out_weight, preferred_element_type=jnp.float32
    )
    mixed_out = (
        taken_together(partial_value.astype(jnp.bfloat16), "tp")
        .astype(jnp.float32)
        .astype(jnp.bfloat16)
    )
    return (mixed_out, log_weight_sum)


def solution(mesh):
    finer = Mesh(
        mesh.devices.reshape(8, 8, mesh.shape["fs"], mesh.shape["tp"]), ("sp_0", "sp_1", "fs", "tp")
    )
    placed = (
        P(FS_SP, None),
        P(),
        P(None, ("tp", "fs")),
        P(None, ("tp", "fs")),
        P(None, ("tp", "fs")),
        P(None, ("tp", "fs")),
        P(None, ("tp", "fs")),
        P(None, ("tp", "fs")),
        P("tp"),
        P("tp", None),
        P(FS_SP),
        P(),
        P(),
        P("tp", None),
        P("tp", None),
    )
    return jax.shard_map(
        on_device,
        mesh=finer,
        in_specs=placed,
        out_specs=(P(FS_SP, None), P("tp", FS_SP)),
        check_vma=False,
    )
```

profile of v0, /device:TPU:1, one launch (start us, length us, event | category | flops | bytes accessed | tf_op | source)
XLA Modules:
  0.0 367.2 jit_solution(1742700413866512903)
XLA Ops:
  7.2 0.0 all-gather.7.cloned.1.call-start
  7.3 1.1 bitcast_dynamic-update-slice_fusion.5
  8.3 1.0 bitcast_dynamic-update-slice_fusion.4
  9.3 1.0 bitcast_dynamic-update-slice_fusion.3
  10.3 1.0 bitcast_dynamic-update-slice_fusion.2
  11.3 1.0 bitcast_dynamic-update-slice_fusion.1
  12.2 1.0 bitcast_dynamic-update-slice_fusion
  13.2 1.1 copy-done.2
  14.3 0.0 all-gather.7.cloned.1.call-update
  14.4 0.0 all-gather.13.cloned.1.call-start
  14.5 0.2 fusion.42
  14.7 76.1 %all-gather.7.cloned.1.call-done = bf16[2048,6,256]{0,2,1:T(8,128)(2,1)} async-done(((bf16[2048,6,64]{0,2,1:T(8,128)(2,1)}), bf16[2048,6,256]{0,2,1:T(8,128)(2,1)}) %all-gather.7.cloned.1.call-update) | async-done | bytes 6291472 | tf_op jit(solution)/shard_map/all_gather | solution.py:163
  90.8 5.0 %convolution_convert_fusion = bf16[128,6,256]{2,0,1:T(8,128)(2,1)S(1)} fusion(bf16[2048,6,256]{0,2,1:T(8,128)(2,1)} %all-gather.7.cloned.1.call-done, bf16[128,2048]{1,0:T(8,128)(2,1)S(1)} %copy-done.3, f32[2048]{0:T(1024)S(1)} %copy-done.5, f32[128]{0:T(128)S(1)} %add_rsqrt_fusion.2), kind=kOutput, calls=%fused_computation.55 | convolution fusion | flops 806551552 | bytes 7217664 | tf_op jit(solution)/shard_map/rd,dnc->rnc/dot_general | solution.py:160
  95.9 0.1 reshape.180
  96.0 0.1 reshape.182
  96.1 0.1 reshape.183
  96.2 0.1 exponential_subtract_fusion
  96.3 16.1 %while.13 = (s32[]{:T(128)}, f32[2,128,128]{2,1,0:T(8,128)S(1)}, f32[2,2,64,128]{3,2,0,1:T(8,128)S(1)}, f32[2,2,64,128]{3,2,0,1:T(8,128)S(1)}, f32[2,2,64,128]{3...) while((s32[]{:T(128)}, f32[2,128,128]{2,1,0:T(8,128)S(1)}, ...), condition=%wide.region_8.9_spmd.clone, body=%wide.region_6.8_spmd.clone.sunk | while | flops 79876096 | bytes 1819267 | solution.py:97
  96.4 0.1 reduce_window_sum.25
  96.5 6.9 %fusion.202 = f32[2,64,1,64]{3,2,1,0:T(1,128)S(1)} fusion(f32[2,64,128,1]{2,3,1,0:T(1,128)S(1)} %bitcast.358, f32[2,64,128]{2,1,0:T(8,128)S(1)} %get-tuple-element.238, f32[2,64,128]{2,1,0:T(8,128)S(1)} %reduce_window_sum.25, pred[64,64]{1,0:T(8,128)(4,1)S(1)} %iota_compare_fusion.2), kind=kOutput, calls=%fused_computation.14.clone.1 | convolution fusion | flops 15728640 | bytes 233472 | tf_op jit(solution)/shard_map/while/body/eval_jaxpr/htk,htsk,hsk->hts/dot_general | solution.py:81
  103.4 0.3 fusion.201
  103.7 0.2 fusion.203
  103.9 0.4 convolution_add_fusion.5
  104.4 0.1 reduce_window_sum.25
  104.5 6.9 %fusion.202 = f32[2,64,1,64]{3,2,1,0:T(1,128)S(1)} fusion(f32[2,64,128,1]{2,3,1,0:T(1,128)S(1)} %bitcast.358, f32[2,64,128]{2,1,0:T(8,128)S(1)} %get-tuple-element.238, f32[2,64,128]{2,1,0:T(8,128)S(1)} %reduce_window_sum.25, pred[64,64]{1,0:T(8,128)(4,1)S(1)} %iota_compare_fusion.2), kind=kOutput, calls=%fused_computation.14.clone.1 | convolution fusion | flops 15728640 | bytes 233472 | tf_op jit(solution)/shard_map/while/body/eval_jaxpr/htk,htsk,hsk->hts/dot_general | solution.py:81
  111.4 0.3 fusion.201
  111.7 0.2 fusion.203
  111.9 0.4 convolution_add_fusion.5
  112.4 0.6 copy-done.1
  113.0 0.0 all-gather.11.cloned.1.call-start
  113.1 0.2 reduce_window_sum.22
  113.3 12.4 %all-gather = f32[16,1,128]{2,1,0:T(1,128)S(1)} all-gather(f32[2,1,128]{2,1,0:T(1,128)S(1)} %slice_exponential_fusion), channel_id=2, replica_groups=mesh['sp_0'=8,'sp_1'=8,'fs'=4,'tp'=2] {'sp_1'}, dimensions={0}, use_global_device_ids=true | all-gather | bytes 9216 | tf_op jit(solution)/shard_map/all_gather | solution.py:36
  125.7 24.3 %all-gather.13.cloned.1.call-done = f32[16,128,128]{2,1,0:T(8,128)} async-done(((f32[2,128,128]{2,1,0:T(8,128)}), f32[16,128,128]{2,1,0:T(8,128)}) %all-gather.13.cloned.1.call-update) | async-done | bytes 1048592 | tf_op jit(solution)/shard_map/all_gather | solution.py:36
  150.0 2.3 bitcast_add_fusion
  152.3 0.0 all-gather.11.cloned.1.call-update
  152.3 0.0 all-gather.9.cloned.1.call-start
  152.4 0.7 pad_maximum_fusion
  153.0 0.0 all-gather.9.cloned.1.call-update
  153.1 0.6 slice.141
  154.2 0.1 copy.85
  154.3 0.1 copy.107
  154.4 13.5 %all_gather.27 = f32[8,2,128]{2,1,0:T(2,128)S(1)} all-gather(f32[1,2,128]{2,1,0:T(2,128)S(1)} %get-tuple-element.183), channel_id=1, replica_groups=mesh['sp_0'=8,'sp_1'=8,'fs'=4,'tp'=2] {'sp_0'}, dimensions={0}, use_global_device_ids=true | all-gather | bytes 9216 | tf_op jit(solution)/shard_map/all_gather | solution.py:36
  168.0 25.6 %all-gather.11.cloned.1.call-done = f32[8,2,128,128]{3,2,1,0:T(8,128)} async-done(((f32[1,2,128,128]{3,2,1,0:T(8,128)}), f32[8,2,128,128]{3,2,1,0:T(8,128)}) %all-gather.11.cloned.1.call-update) | async-done | bytes 1048592 | tf_op jit(solution)/shard_map/all_gather | solution.py:36
  193.5 2.6 multiply_reduce_fusion
  196.2 0.1 multiply_convert_fusion
  196.3 102.3 %all-gather.9.cloned.1.call-done = bf16[8192,512]{1,0:T(8,128)(2,1)} async-done(((bf16[128,512]{1,0:T(8,128)(2,1)}), bf16[8192,512]{1,0:T(8,128)(2,1)}) %all-gather.9.cloned.1.call-update) | async-done | bytes 8388624 | tf_op jit(solution)/shard_map/all_gather | solution.py:21
  298.6 0.4 ge.22
  299.0 53.7 %conditional.1 = (f32[2,2,128]{2,1,0:T(2,128)S(1)}, f32[2,2,128,128]{3,2,1,0:T(8,128)S(1)}, f32[2,128]{1,0:T(2,128)S(1)}) conditional(s32[]{:T(128)} %bitcast.8, () %tuple.22, (s32[]{:T(128)}, s32[128,1]{0,1:T(1,128)S(1)}, s32[128,8192]{1,0:T(8,128)S(1)}, bf16[8192,512]{1,0:T(8,128)(2,1)}, bf16[2,2,128,64]{2,3,1,0:T(8,128)(2,1)S(1)}) %tuple.88), branch_computations={%region_1.0_spmd, %region_2.5_spmd} | conditional | flops 1657798272 | bytes 109395480 | solution.py:178
  299.2 0.7 broadcast_compare_fusion
  299.9 11.9 %copy.86 = bf16[8192,512]{0,1:T(8,128)(2,1)} copy(bf16[8192,512]{1,0:T(8,128)(2,1)} %get-tuple-element.135) | data formatting | bytes 16777216 | tf_op jit(solution)/shard_map
  311.8 5.9 %fusion.173 = (bf16[8192,256]{0,1:T(8,128)(2,1)}, bf16[8192,256]{0,1:T(8,128)(2,1)}) fusion(bf16[8192,512]{0,1:T(8,128)(2,1)} %copy.86), kind=kLoop, calls=%fused_computation.242 | loop fusion | bytes 16777216 | tf_op jit(solution)/shard_map/split | solution.py:22
  317.8 6.3 %copy.84 = bf16[8192,2,128]{2,0,1:T(8,128)(2,1)} copy(bf16[8192,2,128]{0,2,1:T(8,128)(2,1)} %bitcast.357) | data formatting | bytes 8388608 | tf_op jit(solution)/shard_map/cond/branch_1_fun/reshape | solution.py:113
  324.1 11.2 %fusion.2 = (f32[2,2,128]{2,1,0:T(2,128)S(1)}, f32[2,2,128,8192]{3,2,1,0:T(8,128)}) fusion(pred[128,8192]{1,0:T(8,128)(4,1)S(1)} %broadcast_compare_fusion, bf16[2,2,128,64]{2,3,1,0:T(8,128)(2,1)S(1)} %get-tuple-element.54, bf16[2,2,8192,64]{2,3,1,0:T(8,128)(2,1)} %bitcast.361), kind=kOutput, calls=%fused_computation.3 | convolution fusion | flops 549453312 | bytes 22087680 | tf_op jit(solution)/shard_map/cond/branch_1_fun/hmqd,hmkd->hmqk/dot_general | solution.py:114
  335.3 9.3 %fusion.5 = f32[2,2,128,128]{3,2,1,0:T(8,128)S(1)} fusion(f32[2,2,128,8192]{3,2,1,0:T(8,128)} %get-tuple-element.165, f32[2,2,128]{2,1,0:T(2,128)S(1)} %broadcast_maximum_fusion, pred[128,8192]{1,0:T(8,128)(4,1)S(1)} %broadcast_compare_fusion, bf16[8192,2,128]{2,0,1:T(8,128)(2,1)} %copy.84), kind=kOutput, calls=%fused_computation.6 | convolution fusion | flops 1090519040 | bytes 22284288 | tf_op jit(solution)/shard_map/cond/branch_1_fun/itap,ipn->itan/dot_general | solution.py:121
  344.6 8.1 %fusion.4 = f32[2,2,128]{2,1,0:T(2,128)S(1)} fusion(f32[2,2,128,8192]{3,2,1,0:T(8,128)} %get-tuple-element.165, f32[2,2,128]{2,1,0:T(2,128)S(1)} %broadcast_maximum_fusion, pred[128,8192]{1,0:T(8,128)(4,1)S(1)} %broadcast_compare_fusion), kind=kLoop, calls=%fused_computation.5 | loop fusion | flops 16776704 | bytes 17829888 | tf_op jit(solution)/shard_map/cond/branch_1_fun/reduce_sum | solution.py:120
  352.7 0.1 copy.87
  352.9 0.6 log_add_fusion
  353.4 0.1 multiply_reduce_fusion.1
  353.6 0.1 multiply_convert_fusion.1
  353.7 0.3 fusion.174
  354.0 0.3 fusion.41
  354.3 0.1 broadcast_in_dim.46
  354.5 5.1 %all_to_all.5 = bf16[2,128,2048]{2,1,0:T(8,128)(2,1)S(1)} all-to-all(bf16[2,128,2048]{2,1,0:T(8,128)(2,1)S(1)} %broadcast_in_dim.46), channel_id=1, replica_groups=mesh['sp_0'=8,'sp_1'=8,'fs'=4,'tp'=2] {'tp'}, dimensions={0} | all-to-all | bytes 2097152 | tf_op jit(solution)/shard_map/all_to_all | solution.py:48
  359.6 1.1 reduce_sum.51
  (55 shorter events, 0.4 us)
Async XLA Ops:
  7.2 346.5 %copy-start = (bf16[256,2048]{1,0:T(8,128)(2,1)S(1)}, bf16[256,2048]{1,0:T(8,128)(2,1)}, u32[]{:S(2)}) copy-start(bf16[256,2048]{1,0:T(8,128)(2,1)} %param.32) | copy-start | bytes 3145732
  7.2 7.3 %copy-start.3 = (bf16[128,2048]{1,0:T(8,128)(2,1)S(1)}, bf16[128,2048]{1,0:T(8,128)(2,1)}, u32[]{:S(2)}) copy-start(bf16[128,2048]{1,0:T(8,128)(2,1)} %param.19) | copy-start | bytes 1572868
  7.2 7.5 %copy-start.6 = (f32[2,128]{1,0:T(2,128)S(1)}, f32[2,128]{1,0:T(2,128)}, u32[]{:S(2)}) copy-start(f32[2,128]{1,0:T(2,128)} %param.28) | copy-start | bytes 3076
  7.2 83.6 %copy-start.5 = (f32[2048]{0:T(1024)S(1)}, f32[2048]{0:T(1024)}, u32[]{:S(2)}) copy-start(f32[2048]{0:T(1024)} %param.20) | copy-start | bytes 24580
  7.2 83.6 %all-gather.7.cloned.1.call-start = ((), (), s32[]{:S(2)}) async-start(), calls=%async_computation.1 | async-start | bytes 7864320 | tf_op jit(solution)/shard_map/all_gather | solution.py:163
  13.2 1.1 copy-start.2
  14.4 135.6 %all-gather.13.cloned.1.call-start = ((), (), s32[]{:S(2)}) async-start(), calls=%async_computation.4 | async-start | bytes 1179648 | tf_op jit(solution)/shard_map/all_gather | solution.py:36
  14.7 81.5 %copy-start.7 = (f32[128]{0:T(128)S(1)}, f32[128]{0:T(128)}, u32[]{:S(2)}) copy-start(f32[128]{0:T(128)} %param.29) | copy-start | bytes 1540
  112.4 0.7 copy-start.1
  112.4 83.8 %copy-start.8 = (f32[128]{0:T(128)S(1)}, f32[128]{0:T(128)}, u32[]{:S(2)}) copy-start(f32[128]{0:T(128)} %param.31) | copy-start | bytes 1540
  113.0 80.5 %all-gather.11.cloned.1.call-start = ((), (), s32[]{:S(2)}) async-start(), calls=%async_computation.3 | async-start | bytes 1179648 | tf_op jit(solution)/shard_map/all_gather | solution.py:36
  152.3 146.3 %all-gather.9.cloned.1.call-start = ((), (), s32[]{:S(2)}) async-start(), calls=%async_computation.2 | async-start | bytes 8519680 | tf_op jit(solution)/shard_map/all_gather | solution.py:21
  299.0 54.5 %copy-start.9 = (f32[2]{0:T(128)S(1)}, f32[2]{0:T(128)}, u32[]{:S(2)}) copy-start(f32[2]{0:T(128)} %param.27) | copy-start | bytes 28
  299.0 54.6 %copy-start.10 = (f32[128]{0:T(128)S(1)}, f32[128]{0:T(128)}, u32[]{:S(2)}) copy-start(f32[128]{0:T(128)} %param.30) | copy-start | bytes 1540
  299.0 55.0 %copy-start.4 = (bf16[256,2048]{1,0:T(8,128)(2,1)S(1)}, bf16[256,2048]{1,0:T(8,128)(2,1)}, u32[]{:S(2)}) copy-start(bf16[256,2048]{1,0:T(8,128)(2,1)} %param.33) | copy-start | bytes 3145732
Sparse Core Ops, SparseCore 0:
  14.5 76.2 all-gather.6
  113.2 36.8 all-gather.12
  152.4 41.0 all-gather.10
  197.0 101.4 all-gather.8
where the time goes:
time: 368 us; the launch traced here: 367 us
  waiting for transfers between devices  228 us (62%)
  matrix products  44.4 us (12%)
  local copies, waits for them, and re-layouts  33.7 us (9%)
  blocking collectives  31 us (8%)
  between operations  14.8 us (4%)
  other arithmetic  14.5 us (4%)
    all_gather x1, waiting for transfers between devices, in_one_piece(): filled = lax.all_gather(both, axis, axis=dim, tiled=True)  102 us
    all_gather x1, waiting for transfers between devices, on_device(): lax.all_gather(stacked, 'fs', axis=2, tiled=True)  76.1 us
    all_gather x2, waiting for transfers between devices, entering(): pieces = jax.tree.map(lambda part: lax.all_gather(part, axis), running)  49.9 us
    all_gather x2, blocking collectives, entering(): pieces = jax.tree.map(lambda part: lax.all_gather(part, axis), running)  25.9 us
    dot_general x2, matrix products, advance(): jnp.einsum('htk,htsk,hsk->hts', query_block, decay, key_block, precision=...  13.9 us
    another operation x1, local copies, waits for them, and re-layouts  11.9 us
    dot_general x1, matrix products, attend(): jnp.einsum('hmqd,hmkd->hmqk', queries, key_heads, preferred_element_type=...  11.2 us
    dot_general x1, matrix products, attend(): jnp.einsum('itap,ipn->itan', weights.astype(jnp.bfloat16), head_values, p...  9.28 us
  transfers between devices with their start and end apart: 4, of which 4 were waited for; matrix products, arithmetic and copies ran while one was open for 1% of the time, Pallas kernels for 0%

commit v1 on v0

v1 whole, which is shorter than its diff:
```python
import math

import jax
import jax.numpy as jnp
from jax import lax
from jax.experimental import pallas as pl
from jax.experimental.pallas import tpu as pltpu
from jax.sharding import Mesh
from jax.sharding import PartitionSpec as P

DK = 64
DV = 128
ROWS = 128
HALF = 64
SUB = 16
EPS = 1e-06
NEG = -1e30
LOCAL_HEADS = 2
F32 = jnp.float32
BF16 = jnp.bfloat16
HIGHEST = lax.Precision.HIGHEST

VMEM = pl.BlockSpec(memory_space=pltpu.VMEM)
SMEM = pl.BlockSpec(memory_space=pltpu.SMEM)


def dot(a, b, dims, precision=None):
    return lax.dot_general(a, b, (dims, ((), ())), precision=precision, preferred_element_type=F32)


def dot_nn(a, b, precision=None):
    return dot(a, b, ((1,), (0,)), precision)


def dot_nt(a, b):
    return dot(a, b, ((1,), (1,)))


def dot_tn(a, b):
    return dot(a, b, ((0,), (0,)))


def in_parts(x):
    high = x.astype(BF16).astype(F32)
    rest = x - high
    mid = rest.astype(BF16).astype(F32)
    return high, mid, rest - mid


def rows_to_block(rows, count=16):
    at = lax.broadcasted_iota(jnp.int32, (count, ROWS), 0)
    block = jnp.zeros((count, ROWS), F32)
    for r, row in enumerate(rows):
        block = jnp.where(at == r, row, block)
    return block


def swap_halves(a, b):
    low = lax.broadcasted_iota(jnp.int32, a.shape, 1) < HALF
    first = jnp.where(low, a, pltpu.roll(b, HALF, 1))
    second = jnp.where(low, pltpu.roll(a, HALF, 1), b)
    return first, second


def project_kernel(idx, t0, t1, t2, t3, own, peer, out):
    x, c = idx[2], idx[3]
    rows = jnp.concatenate([t0[...], t1[...], t2[...], t3[...]], axis=0)
    for which, weight in ((c, own), (1 - c, peer)):
        result = dot_nn(rows, weight[...]).astype(BF16)
        for k in range(4):
            seq = lax.rem(x - k + 4, 4)
            out[seq * 2 + which] = result[k * HALF : (k + 1) * HALF]


def gates_kernel(ny, idx, raw, scale, bound, slots, kv_own, decayed_q, local_out):
    width = DV // ny
    y_odd = lax.rem(idx[1], 2) == 1
    row = lax.broadcasted_iota(jnp.int32, (ROWS, ROWS), 0)
    lane = lax.broadcasted_iota(jnp.int32, (ROWS, ROWS), 1)
    lane_sub = lax.broadcasted_iota(jnp.int32, (SUB, ROWS), 1)
    row_sub = lax.broadcasted_iota(jnp.int32, (SUB, ROWS), 0)
    lower = (row >= lane).astype(F32)

    def both(head, offset):
        first = raw[4 * head : 4 * head + 2, :, offset : offset + ROWS].reshape(ROWS, ROWS)
        second = raw[4 * head + 2 : 4 * head + 4, :, offset : offset + ROWS].reshape(ROWS, ROWS)
        return swap_halves(first.astype(F32), second.astype(F32))

    keys, values, ends = [], [], []
    for head in range(LOCAL_HEADS):
        k, v = both(head, 0)
        q, rq = both(head, ROWS)
        rf, ri = both(head, 2 * ROWS)
        keys.append(k)
        values.append(v)
        edge = bound[head : head + 1, :]
        forget = edge + (1.0 - edge) * jax.nn.sigmoid(rf)
        log_forget = scale[...] * jnp.log(forget)
        key_in = 1.0 - jnp.exp(log_forget)
        total = dot_nn(lower, log_forget, HIGHEST)
        end = total[ROWS - 1 : ROWS, :]
        ends.append(end)
        ri16 = ri.astype(BF16)
        state_t = dot_tn(ri16, (key_in * jnp.exp(jnp.minimum(end - total, 0.0))).astype(BF16))
        decayed_q[head] = (rq * jnp.exp(total)).astype(BF16)
        strips = []
        for i in range(ROWS // SUB):
            at = slice(i * SUB, (i + 1) * SUB)
            total_i, rq_i, key_i = total[at], rq[at], key_in[at]
            strip = jnp.zeros((SUB, ROWS), F32)
            if i:
                start = total[i * SUB - 1 : i * SUB]
                far_q = rq_i * jnp.exp(jnp.minimum(total_i - start, 0.0))
                far_k = key_in * jnp.exp(jnp.minimum(start - total, 0.0))
                far = dot_nt(far_q.astype(BF16), far_k.astype(BF16))
                strip = jnp.where(lane_sub < i * SUB, far, strip)
            for s in range(SUB):
                decay = jnp.exp(jnp.minimum(total_i - total_i[s : s + 1], 0.0))
                near = jnp.sum(rq_i * decay * key_i[s : s + 1], axis=1, keepdims=True)
                strip = jnp.where((lane_sub == i * SUB + s) & (row_sub >= s), near, strip)
            strips.append(strip)
        scores = jnp.concatenate(strips, axis=0)
        local_out[head] = dot_nn(scores.astype(BF16), ri16)
        q16, state16 = q.astype(BF16), state_t.astype(BF16)
        for y in range(ny):
            if y % 2 == head:
                slots[y, 0:ROWS, :] = q16
            low = ROWS + head * width
            slots[y, low : low + width, :] = state16[y * width : (y + 1) * width]
    parts = rows_to_block([part for end in ends for part in in_parts(end)]).astype(BF16)
    for y in range(ny):
        slots[y, ROWS + 2 * width : ROWS + 2 * width + 16, :] = parts
    kv_own[0] = jnp.where(y_odd, keys[1], keys[0]).astype(BF16)
    kv_own[1] = jnp.where(y_odd, values[1], values[0]).astype(BF16)


def summed_parts(block, head):
    block = block.astype(F32)
    at = 3 * head
    return block[at : at + 1] + block[at + 1 : at + 2] + block[at + 2 : at + 3]


def prefix_kernel(ny, nz, got, kv_own, kv_peer, out, before, decay):
    width = DV // ny
    first = kv_peer[0].reshape(ROWS, ROWS).astype(F32)
    second = kv_peer[1].reshape(ROWS, ROWS).astype(F32)
    k, v = swap_halves(first, second)
    k16, v16 = k.astype(BF16), v.astype(BF16)
    states, totals = [], []
    for head in range(LOCAL_HEADS):
        state = jnp.zeros((width, ROWS), F32)
        total = jnp.zeros((1, ROWS), F32)
        for y in range(ny):
            before[y, head] = state
            decay[y, head : head + 1, :] = total
            low = ROWS + head * width
            end = summed_parts(got[y, ROWS + 2 * width : ROWS + 2 * width + 16, :], head)
            state = jnp.exp(end) * state + got[y, low : low + width, :].astype(F32)
            total = total + end
        states.append(state.astype(BF16))
        totals.extend(in_parts(total))
    parts = rows_to_block(totals).astype(BF16)
    for z in range(nz):
        out[z, 0:ROWS, :] = kv_own[0]
        out[z, ROWS : 2 * ROWS, :] = k16
        out[z, 2 * ROWS : 3 * ROWS, :] = kv_own[1]
        out[z, 3 * ROWS : 4 * ROWS, :] = v16
        for head in range(LOCAL_HEADS):
            low = 4 * ROWS + head * width
            out[z, low : low + width, :] = states[head]
        out[z, 4 * ROWS + 2 * width : 4 * ROWS + 2 * width + 16, :] = parts


def attend_kernel(ny, nz, idx, got_q, got_kv, before, decay, out, keys, values_t, scores):
    width = DV // ny
    z, y = idx[0], idx[1]
    stats_at = 2 * ROWS
    state_at = stats_at + 16
    for head in range(LOCAL_HEADS):
        entering = jnp.zeros((width, ROWS), F32)
        for k in range(nz):
            end = summed_parts(got_kv[k, 4 * ROWS + 2 * width : 4 * ROWS + 2 * width + 16, :], head)
            low = 4 * ROWS + head * width
            new = jnp.exp(end) * entering + got_kv[k, low : low + width, :].astype(F32)
            entering = jnp.where(k < z, new, entering)
        for k in range(ny):
            low = state_at + head * width
            state = before[k, head] + jnp.exp(decay[k, head : head + 1, :]) * entering
            out[k, low : low + width, :] = state.astype(BF16)

    pair = 2 * ROWS
    for k in range(nz):
        keys[k * pair : (k + 1) * pair, :] = got_kv[k, 0:pair, :]
        for h in range(2):
            block = got_kv[k, pair + h * ROWS : pair + (h + 1) * ROWS, :]
            at = k * pair + h * ROWS
            values_t[:, at : at + ROWS] = block.astype(F32).T.astype(BF16)

    key_row = lax.broadcasted_iota(jnp.int32, (pair, 1), 0)
    other = y + 1 - 2 * lax.rem(y, 2)
    key_at = jnp.where(key_row < ROWS, y * ROWS + key_row, other * ROWS + key_row - ROWS)
    query_lane = lax.broadcasted_iota(jnp.int32, (1, pair), 1)
    low_lanes = lax.broadcasted_iota(jnp.int32, (pair, ROWS), 1) < HALF
    scale = DK ** (-0.5)
    for group in range(ny // 2):
        q = jnp.concatenate([got_q[2 * group, 0:ROWS, :], got_q[2 * group + 1, 0:ROWS, :]], axis=0)
        q = q.astype(F32) * scale
        query_at = z * (ny * ROWS) + group * pair + query_lane
        stats = []
        for m in range(2):
            q_map = jnp.where(low_lanes == (m == 0), q, 0.0).astype(BF16)
            highest = jnp.full((8, pair), NEG, F32)
            for k in range(nz):
                part = dot_nt(keys[k * pair : (k + 1) * pair, :], q_map)
                part = jnp.where(key_at + k * (ny * ROWS) <= query_at, part, NEG)
                scores[k * pair : (k + 1) * pair, :] = part
                highest = jnp.maximum(highest, jnp.max(part.reshape(pair // 8, 8, pair), axis=0))
            top = jnp.max(highest, axis=0, keepdims=True)
            summed = jnp.zeros((8, pair), F32)
            numer = jnp.zeros((DV, pair), F32)
            for k in range(nz):
                weights = jnp.exp(scores[k * pair : (k + 1) * pair, :] - top)
                summed = summed + jnp.sum(weights.reshape(pair // 8, 8, pair), axis=0)
                numer = numer + dot_nn(
                    values_t[:, k * pair : (k + 1) * pair], weights.astype(BF16)
                )
            weight_sum = jnp.sum(summed, axis=0, keepdims=True)
            numer = (numer * (1.0 / weight_sum)).astype(BF16)
            stats.append(in_parts(top + jnp.log(weight_sum)))
            for h in range(2):
                cut = slice(h * ROWS, (h + 1) * ROWS)
                out[2 * group + h, m * ROWS : (m + 1) * ROWS, :] = numer[:, cut]
        for h in range(2):
            cut = slice(h * ROWS, (h + 1) * ROWS)
            block = rows_to_block([part[:, cut] for parts in stats for part in parts])
            out[2 * group + h, stats_at : stats_at + 16, :] = block.astype(BF16)


def combine_kernel(
    ny, mix, got, decayed_q, local_out, att_gain, rec_gain, w_att, w_rec, partial, log_sum
):
    width = DV // ny
    stats_at = 2 * ROWS
    state_at = stats_at + 16
    att_heads, rec_heads = [], []
    for head in range(LOCAL_HEADS):
        sources = [k for k in range(ny) if k % 2 == head]
        maps = []
        for m in range(2):
            logs = [summed_parts(got[k, stats_at : stats_at + 16, :], m) for k in sources]
            top = logs[0]
            for entry in logs[1:]:
                top = jnp.maximum(top, entry)
            shares = [jnp.exp(entry - top) for entry in logs]
            total = shares[0]
            for share in shares[1:]:
                total = total + share
            if m == 0:
                log_sum[head : head + 1, :] = top + jnp.log(total)
            inverse = 1.0 / total
            merged = jnp.zeros((DV, ROWS), F32)
            for k, share in zip(sources, shares):
                numer = got[k, m * ROWS : (m + 1) * ROWS, :].astype(F32)
                merged = merged + numer * (share * inverse)
            maps.append(merged)
        att = maps[0] - mix[head] * maps[1]
        att = att * lax.rsqrt(jnp.mean(att * att, axis=0, keepdims=True) + EPS)
        att_heads.append((att.T * att_gain[...] * 0.8).astype(BF16))
        low = state_at + head * width
        state_t = jnp.concatenate([got[k, low : low + width, :] for k in range(ny)], axis=0)
        rec = local_out[head] + dot_nt(decayed_q[head], state_t)
        rec = rec * lax.rsqrt(jnp.mean(rec * rec, axis=1, keepdims=True) + EPS)
        rec_heads.append((rec * rec_gain[...]).astype(BF16))
    att_rows = jnp.concatenate(att_heads, axis=1)
    rec_rows = jnp.concatenate(rec_heads, axis=1)
    result = dot_nn(att_rows, w_att[...]) + dot_nn(rec_rows, w_rec[...])
    partial[...] = result.astype(BF16)


def ring(size, step):
    return [(i, (i + step) % size) for i in range(size)]


def on_device(ny, nz, *args):
    (tokens, in_gain, wq, wk, wv, wrq, wrf, wri, mix_lambda, lower_bound) = args[:10]
    (forget_scale, att_gain, recurrence_gain, att_out_weight, rec_out_weight) = args[10:]
    z, y, x, c = (lax.axis_index(name) for name in ("z", "y", "x", "c"))
    idx = jnp.stack([z, y, x, c]).astype(jnp.int32)
    width = DV // ny
    d_model = tokens.shape[1]

    rows = lax.dynamic_slice_in_dim(tokens, c * HALF, HALF, 0).astype(F32)
    mean_square = jnp.mean(rows * rows, axis=-1, keepdims=True)
    normed = (rows * lax.rsqrt(mean_square + EPS) * in_gain).astype(BF16)
    gathered = [normed] + [lax.ppermute(normed, "x", ring(4, k)) for k in (1, 2, 3)]
    own = jnp.concatenate([wk, wv, wq, wrq, wrf, wri], axis=1)
    peer = lax.ppermute(own, "c", ring(2, 1))

    projected = pl.pallas_call(
        project_kernel,
        out_shape=jax.ShapeDtypeStruct((8, HALF, 384), BF16),
        in_specs=[SMEM] + [VMEM] * 6,
        out_specs=VMEM,
        name="project",
    )(idx, *gathered, own, peer)
    raw = lax.all_to_all(projected, ("x", "c"), 0, 0, tiled=True)

    other_head = 1 - lax.rem(y, 2)
    kv_send = lax.dynamic_slice(
        raw.reshape(4, 2, HALF, 384), (2 * other_head, 0, 0, 0), (2, 2, HALF, ROWS)
    )
    kv_peer = lax.ppermute(kv_send, "y", [(i, i ^ 1) for i in range(ny)])

    slots, kv_own, decayed_q, local_out = pl.pallas_call(
        lambda *refs: gates_kernel(ny, *refs),
        out_shape=(
            jax.ShapeDtypeStruct((ny, ROWS + 2 * width + 16, ROWS), BF16),
            jax.ShapeDtypeStruct((2, ROWS, ROWS), BF16),
            jax.ShapeDtypeStruct((LOCAL_HEADS, ROWS, ROWS), BF16),
            jax.ShapeDtypeStruct((LOCAL_HEADS, ROWS, ROWS), F32),
        ),
        in_specs=[SMEM, VMEM, VMEM, VMEM],
        out_specs=(VMEM,) * 4,
        name="gates",
    )(idx, raw, forget_scale.reshape(ROWS, 1), lower_bound)
    got_q = lax.all_to_all(slots, "y", 0, 0, tiled=True)

    kv_slots, before, decay = pl.pallas_call(
        lambda *refs: prefix_kernel(ny, nz, *refs),
        out_shape=(
            jax.ShapeDtypeStruct((nz, 4 * ROWS + 2 * width + 16, ROWS), BF16),
            jax.ShapeDtypeStruct((ny, LOCAL_HEADS, width, ROWS), F32),
            jax.ShapeDtypeStruct((ny, LOCAL_HEADS, ROWS), F32),
        ),
        in_specs=[VMEM] * 3,
        out_specs=(VMEM,) * 3,
        name="prefix",
    )(got_q, kv_own, kv_peer)
    got_kv = lax.all_to_all(kv_slots, "z", 0, 0, tiled=True)

    keys_in_all = nz * 2 * ROWS
    results = pl.pallas_call(
        lambda *refs: attend_kernel(ny, nz, *refs),
        out_shape=jax.ShapeDtypeStruct((ny, 2 * ROWS + 16 + 2 * width, ROWS), BF16),
        in_specs=[SMEM] + [VMEM] * 4,
        out_specs=VMEM,
        scratch_shapes=[
            pltpu.VMEM((keys_in_all, ROWS), BF16),
            pltpu.VMEM((DV, keys_in_all), BF16),
            pltpu.VMEM((keys_in_all, 2 * ROWS), F32),
        ],
        name="attend",
    )(idx, got_q, got_kv, before, decay)
    returned = lax.all_to_all(results, "y", 0, 0, tiled=True)

    partial, log_weight_sum = pl.pallas_call(
        lambda *refs: combine_kernel(ny, *refs),
        out_shape=(
            jax.ShapeDtypeStruct((ROWS, d_model), BF16),
            jax.ShapeDtypeStruct((LOCAL_HEADS, ROWS), F32),
        ),
        in_specs=[SMEM] + [VMEM] * 7,
        out_specs=(VMEM, VMEM),
        name="combine",
    )(
        mix_lambda,
        returned,
        decayed_q,
        local_out,
        att_gain.reshape(1, DV),
        recurrence_gain.reshape(1, DV),
        att_out_weight,
        rec_out_weight,
    )
    other = lax.ppermute(partial, "c", ring(2, 1))
    mixed_out = (partial.astype(F32) + other.astype(F32)).astype(BF16)
    return mixed_out, log_weight_sum


def solution(mesh):
    side = math.isqrt(mesh.shape["sp"])
    finer = Mesh(
        mesh.devices.reshape(side, side, mesh.shape["fs"], mesh.shape["tp"]), ("z", "y", "x", "c")
    )
    rows = ("x", "z", "y")
    columns = P(None, ("c", "x"))
    placed = (P(rows, None), P()) + (columns,) * 6
    placed += (P("c"), P("c", None), P(rows), P(), P(), P("c", None), P("c", None))
    return jax.shard_map(
        lambda *args: on_device(side, side, *args),
        mesh=finer,
        in_specs=placed,
        out_specs=(P(rows, None), P("c", rows)),
        check_vma=False,
    )
```

time: 368 us -> 164 us (0.45)
  waiting for transfers between devices: 228 us -> 27.4 us
  matrix products: 44.4 us -> 0 us
  starting transfers between devices: 0.16 us -> 36 us
  blocking collectives: 31 us -> 55.4 us
  Pallas kernels: 0 us -> 23.3 us
  local copies, waits for them, and re-layouts: 33.7 us -> 15.4 us
  between operations: 14.8 us -> 0.85 us
  other arithmetic: 14.5 us -> 4.83 us
    all_gather x4 -> x0, waiting for transfers between devices: 228 us -> none  [the longest x1 102 us: in_one_piece(): filled = lax.all_gather(both, axis, axis=dim, tiled=True)]
    all_to_all x1 -> x2, blocking collectives: 5.13 us -> 55.4 us  [the longest x1 35 us: on_device(): got_kv = lax.all_to_all(kv_slots, 'z', 0, 0, tiled=True)]
    dot_general x14 -> x0, matrix products: 44.4 us -> none  [the longest x2 13.9 us: advance(): jnp.einsum('htk,htsk,hsk->hts', query_block, decay, key_block, precision=...]
    ppermute x0 -> x6, starting transfers between devices: none -> 27.5 us  [the longest x1 8.75 us: on_device(): peer = lax.ppermute(own, 'c', ring(2, 1))]
    all_gather x2 -> x0, blocking collectives: 25.9 us -> none  [entering(): pieces = jax.tree.map(lambda part: lax.all_gather(part, axis), running)]
    pallas_call x0 -> x5, Pallas kernels: none -> 23.3 us  [the longest x1 10 us: on_device(): pl.pallas_call(lambda *refs: attend_kernel(ny, nz, *refs), out_shape=jax....]
    ppermute x0 -> x6, waiting for transfers between devices: none -> 17.3 us  [the longest x3 9.81 us: on_device(): lax.ppermute(normed, 'x', ring(4, k))]
    another operation x2 -> x0, local copies, waits for them, and re-layouts: 12.9 us -> none
  transfers between devices with their start and end apart: 4 -> 8, of which waited for: 4 -> 6; matrix products, arithmetic and copies ran while one was open for 1% -> 3% of each run, Pallas kernels for 0% -> 0%
where the time goes in v1:
time: 164 us; the launch traced here: 163 us
  blocking collectives  55.4 us (34%)
  starting transfers between devices  36 us (22%)
  waiting for transfers between devices  27.4 us (17%)
  Pallas kernels  23.3 us (14%)
  local copies, waits for them, and re-layouts  15.4 us (9%)
  other arithmetic  4.83 us (3%)
    all_to_all x1, blocking collectives, on_device(): got_kv = lax.all_to_all(kv_slots, 'z', 0, 0, tiled=True)  35 us
    all_to_all x1, blocking collectives, on_device(): returned = lax.all_to_all(results, 'y', 0, 0, tiled=True)  20.4 us
    pallas_call x1, Pallas kernels, on_device(): pl.pallas_call(lambda *refs: attend_kernel(ny, nz, *refs), out_shape=jax....  10 us
    ppermute x3, waiting for transfers between devices, on_device(): lax.ppermute(normed, 'x', ring(4, k))  9.81 us
    ppermute x1, starting transfers between devices, on_device(): peer = lax.ppermute(own, 'c', ring(2, 1))  8.75 us
    unnamed x30, local copies, waits for them, and re-layouts  8.51 us
    ppermute x3, starting transfers between devices, on_device(): lax.ppermute(normed, 'x', ring(4, k))  8.42 us
    ppermute x1, starting transfers between devices, on_device(): other = lax.ppermute(partial, 'c', ring(2, 1))  7.13 us
  transfers between devices with their start and end apart: 8, of which 6 were waited for; matrix products, arithmetic and copies ran while one was open for 3% of the time, Pallas kernels for 0%

profile of v1, /device:TPU:1, one launch (start us, length us, event | category | flops | bytes accessed | tf_op | source)
XLA Modules:
  0.0 163.2 jit_solution(6046962318244354002)
XLA Ops:
  0.6 0.0 copy-start.5
  0.6 0.0 copy-start.6
  0.7 0.0 copy-start.7
  0.7 1.3 copy.17
  2.0 0.0 copy-start.8
  2.0 1.3 copy.18
  3.2 0.0 copy-done.5
  3.3 0.3 copy.19
  3.5 0.0 copy-done.6
  3.5 1.0 copy.20
  4.5 0.0 copy-done.7
  4.5 1.0 copy.21
  5.6 0.0 copy-done.8
  5.6 1.0 copy.22
  6.6 0.0 copy-start.10
  6.6 5.3 %concatenate.3.own = bf16[2048,384]{1,0:T(8,128)(2,1)S(1)} concatenate(bf16[2048,64]{1,0:T(8,128)(2,1)S(1)} %copy.17, bf16[2048,64]{1,0:T(8,128)(2,1)S(1)} %copy.18, bf16[2048,64]{1,0:T(8,128)(2,1)S(1)} %copy.19, bf16[2048,64]{1,0:T(8,128)(2,1)} %copy.20, bf16[2048,64]{1,0:T(8,128)(2,1)} %copy.21, bf16[2048,64]{1,0:T(8,128)(2,1)} %copy.22), dimensions={1} | concatenate | bytes 3145728 | tf_op jit(solution)/shard_map/concatenate | solution.py:296
  11.8 0.0 copy-start
  11.8 8.7 %collective-permute-start.3 = (bf16[2048,384]{1,0:T(8,128)(2,1)S(1)}, bf16[2048,384]{1,0:T(8,128)(2,1)S(1)}, u32[]{:S(2)}, u32[]{:S(2)}) collective-permute-start(bf16[2048,384]{1,0:T(8,128)(2,1)S(1)} %concatenate.3.own), channel_id=1, source_target_pairs={{0,1},{1,0},{2,3},{3,2},{4,5},{5,4},{6,7},{7,6},{8,9},{9,8},{10,11... | collective-permute-start | bytes 4718600 | tf_op jit(solution)/shard_map/ppermute | solution.py:297
  20.6 1.1 fusion
  21.7 0.0 copy-done.10
  21.7 1.1 fusion.2.t0
  22.8 0.0 copy-start.4
  22.8 1.9 %collective-permute-start = (bf16[64,2048]{1,0:T(8,128)(2,1)S(1)}, bf16[64,2048]{1,0:T(8,128)(2,1)}, u32[]{:S(2)}, u32[]{:S(2)}) collective-permute-start(bf16[64,2048]{1,0:T(8,128)(2,1)S(1)} %fusion.2.t0), channel_id=1, source_target_pairs={{0,2},{2,4},{4,6},{6,0},{1,3},{3,5},{5,7},{7,1},{8,10},{10,12},{12... | collective-permute-start | bytes 786440 | tf_op jit(solution)/shard_map/ppermute | solution.py:295
  24.8 1.9 %collective-permute-start.1 = (bf16[64,2048]{1,0:T(8,128)(2,1)S(1)}, bf16[64,2048]{1,0:T(8,128)(2,1)}, u32[]{:S(2)}, u32[]{:S(2)}) collective-permute-start(bf16[64,2048]{1,0:T(8,128)(2,1)S(1)} %fusion.2.t0), channel_id=1, source_target_pairs={{0,4},{2,6},{4,0},{6,2},{1,5},{3,7},{5,1},{7,3},{8,12},{10,14},{12... | collective-permute-start | bytes 786440 | tf_op jit(solution)/shard_map/ppermute | solution.py:295
  26.7 4.6 %collective-permute-start.2 = (bf16[64,2048]{1,0:T(8,128)(2,1)S(1)}, bf16[64,2048]{1,0:T(8,128)(2,1)}, u32[]{:S(2)}, u32[]{:S(2)}) collective-permute-start(bf16[64,2048]{1,0:T(8,128)(2,1)S(1)} %fusion.2.t0), channel_id=1, source_target_pairs={{0,6},{2,0},{4,2},{6,4},{1,7},{3,1},{5,3},{7,5},{8,14},{10,8},{12,... | collective-permute-start | bytes 786440 | tf_op jit(solution)/shard_map/ppermute | solution.py:295
  31.3 0.7 pad_add_fusion.idx.refs_0_
  32.0 0.0 copy-start.11
  32.0 7.6 %collective-permute-done.t1 = bf16[64,2048]{1,0:T(8,128)(2,1)} collective-permute-done((bf16[64,2048]{1,0:T(8,128)(2,1)S(1)}, bf16[64,2048]{1,0:T(8,128)(2,1)}, u32[]{:S(2)}, u32[]{:S(2)}) %collective-permute-start) | collective-permute-done | bytes 262176 | tf_op jit(solution)/shard_map/ppermute | solution.py:295
  39.5 0.0 collective-permute-done.1.t2
  39.5 2.3 %collective-permute-done.2.t3 = bf16[64,2048]{1,0:T(8,128)(2,1)} collective-permute-done((bf16[64,2048]{1,0:T(8,128)(2,1)S(1)}, bf16[64,2048]{1,0:T(8,128)(2,1)}, u32[]{:S(2)}, u32[]{:S(2)}) %collective-permute-start.2) | collective-permute-done | bytes 262176 | tf_op jit(solution)/shard_map/ppermute | solution.py:295
  41.8 0.0 collective-permute-done.3.peer
  41.8 0.0 copy-done
  41.8 0.0 copy-done.4
  41.8 0.0 copy-start.3
  41.8 1.1 copy-done.3
  42.9 4.2 %project.1 = bf16[8,64,384]{2,1,0:T(8,128)(2,1)} custom-call(s32[4]{0:T(128)} %pad_add_fusion.idx.refs_0_, bf16[64,2048]{1,0:T(8,128)(2,1)} %copy-done.4, bf16[64,2048]{1,0:T(8,128)(2,1)} %collective-permute-done.t1, bf16[64,2048]{1,0:T(8,128)(2,1)} %collective-permute-done.1.t2, bf16[64,2048]{1,0:T(8,128)(2,1)} %collective-permute-done.2.t3, ...), custom_call_target="tpu_custom_call" | custom-call | tf_op jit(solution)/shard_map/project/pallas_call | solution.py:299
  47.2 5.1 %all-to-all-start = ((bf16[8,64,384]{2,1,0:T(8,128)(2,1)}), bf16[8,64,384]{2,1,0:T(8,128)(2,1)S(1)}, u32[]{:S(2)}, u32[]{:S(2)}) async-start(bf16[8,64,384]{2,1,0:T(8,128)(2,1)} %project.1), calls=%async_computation | async-start | bytes 786432 | tf_op jit(solution)/shard_map/all_to_all | solution.py:306
  52.2 0.0 copy-done.11
  52.2 0.7 copy.23.refs_2_
  53.0 6.9 %all-to-all-done.refs_1_ = bf16[8,64,384]{2,1,0:T(8,128)(2,1)S(1)} async-done(((bf16[8,64,384]{2,1,0:T(8,128)(2,1)}), bf16[8,64,384]{2,1,0:T(8,128)(2,1)S(1)}, u32[]{:S(2)}, u32[]{:S(2)}) %all-to-all-start) | async-done | bytes 393248 | tf_op jit(solution)/shard_map/all_to_all | solution.py:306
  59.9 0.0 copy-start.2
  59.9 0.7 copy-done.2
  60.6 3.4 %gates.1 = (bf16[8,176,128]{2,1,0:T(8,128)(2,1)}, bf16[2,128,128]{2,1,0:T(8,128)(2,1)}, bf16[2,128,128]{2,1,0:T(8,128)(2,1)}, f32[2,128,128]{2,1,0:T(8,128)}) custom-call(s32[4]{0:T(128)} %pad_add_fusion.idx.refs_0_, bf16[8,64,384]{2,1,0:T(8,128)(2,1)} %copy-done.2, f32[128,1]{1,0:T(8,128)} %copy.23.refs_2_, f32[2,128]{1,0:T(2,128)} %refs_3_.1), custom_call_target="tpu_custom_call" | custom-call | tf_op jit(solution)/shard_map/gates/pallas_call | solution.py:314
  64.0 3.4 %all-to-all-start.1 = ((bf16[8,176,128]{2,1,0:T(8,128)(2,1)}), bf16[8,176,128]{2,1,0:T(8,128)(2,1)S(1)}, u32[]{:S(2)}, u32[]{:S(2)}) async-start(bf16[8,176,128]{2,1,0:T(8,128)(2,1)} %get-tuple-element.11), calls=%async_computation.1 | async-start | bytes 720896 | tf_op jit(solution)/shard_map/all_to_all | solution.py:326
  67.5 0.8 constant_dynamic-slice_fusion
  68.3 3.2 %collective-permute-start.4 = (bf16[2,2,64,128]{3,2,1,0:T(8,128)(2,1)S(1)}, bf16[2,2,64,128]{3,2,1,0:T(8,128)(2,1)S(1)}, u32[]{:S(2)}, u32[]{:S(2)}) collective-permute-start(bf16[2,2,64,128]{3,2,1,0:T(8,128)(2,1)S(1)} %constant_dynamic-slice_fusion), channel_id=1, source_target_pairs={{0,8},{8,0},{16,24},{24,16},{32,40},{40,32},{48,56},{56,48},{1,9},... | collective-permute-start | bytes 196616 | tf_op jit(solution)/shard_map/ppermute | solution.py:312
  71.6 5.7 %collective-permute-done.4.refs_2_ = bf16[2,2,64,128]{3,2,1,0:T(8,128)(2,1)S(1)} collective-permute-done((bf16[2,2,64,128]{3,2,1,0:T(8,128)(2,1)S(1)}, bf16[2,2,64,128]{3,2,1,0:T(8,128)(2,1)S(1)}, u32[]{:S(2)}, u32[]{:S(2)}) %collective-permute-start.4) | collective-permute-done | bytes 65568 | tf_op jit(solution)/shard_map/ppermute | solution.py:312
  77.3 0.0 copy-start.9
  77.3 3.2 %all-to-all-done.1.refs_0_.refs_1_ = bf16[8,176,128]{2,1,0:T(8,128)(2,1)S(1)} async-done(((bf16[8,176,128]{2,1,0:T(8,128)(2,1)}), bf16[8,176,128]{2,1,0:T(8,128)(2,1)S(1)}, u32[]{:S(2)}, u32[]{:S(2)}) %all-to-all-start.1) | async-done | bytes 360480 | tf_op jit(solution)/shard_map/all_to_all | solution.py:326
  80.5 0.0 copy-start.1
  80.5 0.0 copy-done.9
  80.5 0.7 copy-done.1
  81.2 2.2 %prefix.1 = (bf16[8,560,128]{2,1,0:T(8,128)(2,1)}, f32[8,2,16,128]{3,2,1,0:T(8,128)}, f32[8,2,128]{2,1,0:T(2,128)}) custom-call(bf16[8,176,128]{2,1,0:T(8,128)(2,1)} %copy-done.1, bf16[2,128,128]{2,1,0:T(8,128)(2,1)} %get-tuple-element.12.refs_1_, bf16[2,2,64,128]{3,2,1,0:T(8,128)(2,1)} %copy-done.9), custom_call_target="tpu_custom_call" | custom-call | tf_op jit(solution)/shard_map/prefix/pallas_call | solution.py:328
  83.4 35.0 %all_to_all.20.refs_2_ = bf16[8,560,128]{2,1,0:T(8,128)(2,1)} all-to-all(bf16[8,560,128]{2,1,0:T(8,128)(2,1)} %get-tuple-element.13), channel_id=1, replica_groups=mesh['z'=8,'y'=8,'x'=4,'c'=2] {'z'}, dimensions={0} | all-to-all | bytes 2293760 | tf_op jit(solution)/shard_map/all_to_all | solution.py:339
  118.5 10.0 %attend.1 = bf16[8,304,128]{2,1,0:T(8,128)(2,1)} custom-call(s32[4]{0:T(128)} %pad_add_fusion.idx.refs_0_, bf16[8,176,128]{2,1,0:T(8,128)(2,1)} %copy-done.1, bf16[8,560,128]{2,1,0:T(8,128)(2,1)} %all_to_all.20.refs_2_, f32[8,2,16,128]{3,2,1,0:T(8,128)} %get-tuple-element.14.refs_3_, f32[8,2,128]{2,1,0:T(2,128)} %get-tuple-element.15.refs_4_), custom_call_target="tpu_custom_call" | custom-call | tf_op jit(solution)/shard_map/attend/pallas_call | solution.py:342
  128.5 20.4 %all_to_all.21.refs_1_ = bf16[8,304,128]{2,1,0:T(8,128)(2,1)} all-to-all(bf16[8,304,128]{2,1,0:T(8,128)(2,1)} %attend.1), channel_id=1, replica_groups=mesh['z'=8,'y'=8,'x'=4,'c'=2] {'y'}, dimensions={0} | all-to-all | bytes 1245184 | tf_op jit(solution)/shard_map/all_to_all | solution.py:354
  148.9 3.5 %combine.1 = (bf16[128,2048]{1,0:T(8,128)(2,1)}, f32[2,128]{1,0:T(2,128)}) custom-call(f32[2]{0:T(128)} %refs_0_.1, bf16[8,304,128]{2,1,0:T(8,128)(2,1)} %all_to_all.21.refs_1_, bf16[2,128,128]{2,1,0:T(8,128)(2,1)} %get-tuple-element.16.refs_2_, f32[2,128,128]{2,1,0:T(8,128)} %get-tuple-element.17.refs_3_, f32[1,128]{1,0:T(1,128)} %bitcast.10, ...), custom_call_target="tpu_custom_call" | custom-call | tf_op jit(solution)/shard_map/combine/pallas_call | solution.py:356
  152.4 7.1 %collective-permute-start.5 = (bf16[128,2048]{1,0:T(8,128)(2,1)}, bf16[128,2048]{1,0:T(8,128)(2,1)S(1)}, u32[]{:S(2)}, u32[]{:S(2)}) collective-permute-start(bf16[128,2048]{1,0:T(8,128)(2,1)} %get-tuple-element.18), channel_id=1, source_target_pairs={{0,1},{1,0},{2,3},{3,2},{4,5},{5,4},{6,7},{7,6},{8,9},{9,8},{10,11... | collective-permute-start | bytes 1572872 | tf_op jit(solution)/shard_map/ppermute | solution.py:375
  159.5 1.7 %collective-permute-done.5 = bf16[128,2048]{1,0:T(8,128)(2,1)S(1)} collective-permute-done((bf16[128,2048]{1,0:T(8,128)(2,1)}, bf16[128,2048]{1,0:T(8,128)(2,1)S(1)}, u32[]{:S(2)}, u32[]{:S(2)}) %collective-permute-start.5) | collective-permute-done | bytes 524320 | tf_op jit(solution)/shard_map/ppermute | solution.py:375
  161.2 2.0 %add_convert_fusion = bf16[128,2048]{1,0:T(8,128)(2,1)} fusion(bf16[128,2048]{1,0:T(8,128)(2,1)S(1)} %collective-permute-done.5, bf16[128,2048]{1,0:T(8,128)(2,1)} %get-tuple-element.18), kind=kLoop, calls=%fused_computation | loop fusion | flops 1048576 | bytes 1572864 | tf_op jit(solution)/shard_map/convert_element_type | solution.py:376
  (1 shorter events, 0.0 us)
Async XLA Ops:
  0.6 2.6 %copy-start.5 = (bf16[2048,64]{0,1:T(8,128)(2,1)S(1)}, bf16[2048,64]{0,1:T(8,128)(2,1)}, u32[]{:S(2)}) copy-start(bf16[2048,64]{0,1:T(8,128)(2,1)} %param.17) | copy-start | bytes 786436
  0.6 2.9 %copy-start.6 = (bf16[2048,64]{0,1:T(8,128)(2,1)S(1)}, bf16[2048,64]{0,1:T(8,128)(2,1)}, u32[]{:S(2)}) copy-start(bf16[2048,64]{0,1:T(8,128)(2,1)} %param.20) | copy-start | bytes 786436
  0.7 3.9 %copy-start.7 = (bf16[2048,64]{0,1:T(8,128)(2,1)S(1)}, bf16[2048,64]{0,1:T(8,128)(2,1)}, u32[]{:S(2)}) copy-start(bf16[2048,64]{0,1:T(8,128)(2,1)} %param.21) | copy-start | bytes 786436
  2.0 3.6 %copy-start.8 = (bf16[2048,64]{0,1:T(8,128)(2,1)S(1)}, bf16[2048,64]{0,1:T(8,128)(2,1)}, u32[]{:S(2)}) copy-start(bf16[2048,64]{0,1:T(8,128)(2,1)} %param.22) | copy-start | bytes 786436
  6.6 15.2 %copy-start.10 = (f32[2048]{0:T(1024)S(1)}, f32[2048]{0:T(1024)}, u32[]{:S(2)}) copy-start(f32[2048]{0:T(1024)} %param.16) | copy-start | bytes 24580
  11.8 29.9 %copy-start = (bf16[2048,384]{1,0:T(8,128)(2,1)}, bf16[2048,384]{1,0:T(8,128)(2,1)S(1)}, u32[]{:S(2)}) copy-start(bf16[2048,384]{1,0:T(8,128)(2,1)S(1)} %concatenate.3.own) | copy-start | bytes 4718596
  11.8 29.9 %collective-permute-start.3 = (bf16[2048,384]{1,0:T(8,128)(2,1)S(1)}, bf16[2048,384]{1,0:T(8,128)(2,1)S(1)}, u32[]{:S(2)}, u32[]{:S(2)}) collective-permute-start(bf16[2048,384]{1,0:T(8,128)(2,1)S(1)} %concatenate.3.own), channel_id=1, source_target_pairs={{0,1},{1,0},{2,3},{3,2},{4,5},{5,4},{6,7},{7,6},{8,9},{9,8},{10,11... | collective-permute-start | bytes 4718600 | tf_op jit(solution)/shard_map/ppermute | solution.py:297
  22.8 19.0 %copy-start.4 = (bf16[64,2048]{1,0:T(8,128)(2,1)}, bf16[64,2048]{1,0:T(8,128)(2,1)S(1)}, u32[]{:S(2)}) copy-start(bf16[64,2048]{1,0:T(8,128)(2,1)S(1)} %fusion.2.t0) | copy-start | bytes 786436
  22.8 16.7 %collective-permute-start = (bf16[64,2048]{1,0:T(8,128)(2,1)S(1)}, bf16[64,2048]{1,0:T(8,128)(2,1)}, u32[]{:S(2)}, u32[]{:S(2)}) collective-permute-start(bf16[64,2048]{1,0:T(8,128)(2,1)S(1)} %fusion.2.t0), channel_id=1, source_target_pairs={{0,2},{2,4},{4,6},{6,0},{1,3},{3,5},{5,7},{7,1},{8,10},{10,12},{12... | collective-permute-start | bytes 786440 | tf_op jit(solution)/shard_map/ppermute | solution.py:295
  24.8 14.8 %collective-permute-start.1 = (bf16[64,2048]{1,0:T(8,128)(2,1)S(1)}, bf16[64,2048]{1,0:T(8,128)(2,1)}, u32[]{:S(2)}, u32[]{:S(2)}) collective-permute-start(bf16[64,2048]{1,0:T(8,128)(2,1)S(1)} %fusion.2.t0), channel_id=1, source_target_pairs={{0,4},{2,6},{4,0},{6,2},{1,5},{3,7},{5,1},{7,3},{8,12},{10,14},{12... | collective-permute-start | bytes 786440 | tf_op jit(solution)/shard_map/ppermute | solution.py:295
  26.7 15.1 %collective-permute-start.2 = (bf16[64,2048]{1,0:T(8,128)(2,1)S(1)}, bf16[64,2048]{1,0:T(8,128)(2,1)}, u32[]{:S(2)}, u32[]{:S(2)}) collective-permute-start(bf16[64,2048]{1,0:T(8,128)(2,1)S(1)} %fusion.2.t0), channel_id=1, source_target_pairs={{0,6},{2,0},{4,2},{6,4},{1,7},{3,1},{5,3},{7,5},{8,14},{10,8},{12,... | collective-permute-start | bytes 786440 | tf_op jit(solution)/shard_map/ppermute | solution.py:295
  32.0 20.2 %copy-start.11 = (f32[128]{0:T(128)S(1)}, f32[128]{0:T(128)}, u32[]{:S(2)}) copy-start(f32[128]{0:T(128)} %param.25) | copy-start | bytes 1540
  41.8 1.1 copy-start.3
  47.2 12.8 %all-to-all-start = ((bf16[8,64,384]{2,1,0:T(8,128)(2,1)}), bf16[8,64,384]{2,1,0:T(8,128)(2,1)S(1)}, u32[]{:S(2)}, u32[]{:S(2)}) async-start(bf16[8,64,384]{2,1,0:T(8,128)(2,1)} %project.1), calls=%async_computation | async-start | bytes 786432 | tf_op jit(solution)/shard_map/all_to_all | solution.py:306
  59.9 0.7 copy-start.2
  64.0 16.5 %all-to-all-start.1 = ((bf16[8,176,128]{2,1,0:T(8,128)(2,1)}), bf16[8,176,128]{2,1,0:T(8,128)(2,1)S(1)}, u32[]{:S(2)}, u32[]{:S(2)}) async-start(bf16[8,176,128]{2,1,0:T(8,128)(2,1)} %get-tuple-element.11), calls=%async_computation.1 | async-start | bytes 720896 | tf_op jit(solution)/shard_map/all_to_all | solution.py:326
  68.3 9.0 %collective-permute-start.4 = (bf16[2,2,64,128]{3,2,1,0:T(8,128)(2,1)S(1)}, bf16[2,2,64,128]{3,2,1,0:T(8,128)(2,1)S(1)}, u32[]{:S(2)}, u32[]{:S(2)}) collective-permute-start(bf16[2,2,64,128]{3,2,1,0:T(8,128)(2,1)S(1)} %constant_dynamic-slice_fusion), channel_id=1, source_target_pairs={{0,8},{8,0},{16,24},{24,16},{32,40},{40,32},{48,56},{56,48},{1,9},... | collective-permute-start | bytes 196616 | tf_op jit(solution)/shard_map/ppermute | solution.py:312
  77.3 3.2 %copy-start.9 = (bf16[2,2,64,128]{3,2,1,0:T(8,128)(2,1)}, bf16[2,2,64,128]{3,2,1,0:T(8,128)(2,1)S(1)}, u32[]{:S(2)}) copy-start(bf16[2,2,64,128]{3,2,1,0:T(8,128)(2,1)S(1)} %collective-permute-done.4.refs_2_) | copy-start | bytes 196612
  80.5 0.7 copy-start.1
  152.4 8.9 %collective-permute-start.5 = (bf16[128,2048]{1,0:T(8,128)(2,1)}, bf16[128,2048]{1,0:T(8,128)(2,1)S(1)}, u32[]{:S(2)}, u32[]{:S(2)}) collective-permute-start(bf16[128,2048]{1,0:T(8,128)(2,1)} %get-tuple-element.18), channel_id=1, source_target_pairs={{0,1},{1,0},{2,3},{3,2},{4,5},{5,4},{6,7},{7,6},{8,9},{9,8},{10,11... | collective-permute-start | bytes 1572872 | tf_op jit(solution)/shard_map/ppermute | solution.py:375
